TPU v7x, 32 devices: a whole 2x2x4 slice. The times are simulated.
32 devices in a mesh: sp: 8 (over z, y), tp: 4 (over x, core).
Axes of the slice: x: 2, y: 2, z: 4, core: 2. Of those that a mesh axis runs over, the one named last changes fastest.
Arguments:
- queries: bfloat16 [4096, 1024], P('sp', 'tp'), may hold values from -200 to 200
- keys: bfloat16 [4096, 1024], P('sp', 'tp'), may hold values from -6 to 6
- values: bfloat16 [4096, 1024], P('sp', 'tp'), may hold values from -24 to 24
- cum_gate: float32 [4096, 8], P('sp', 'tp'), may hold values from -414 to 0, as said below
- residual: bfloat16 [4096, 2048], P(('sp', 'tp')), may hold values from -1.5 to 1.5
- w_out: bfloat16 [1024, 2048], replicated, may hold values from -0.1875 to 0.1875
- gain: float32 [2048], replicated, may hold values from 0.1 to 1.9
- w_up: bfloat16 [2048, 8192], P('sp', 'tp'), may hold values from -0.125 to 0.125
- w_down: bfloat16 [8192, 2048], P('tp', 'sp'), may hold values from -0.0625 to 0.0625
Outputs:
- output: bfloat16 [4096, 2048], P(('sp', 'tp'))
Inputs may be any that keep to these rules, and one draw needn't show every extreme that they name: Within each head, cum_gate never rises from one position to the next.
All inputs are finite; a program needn't handle non-finite values.
Results may differ from a plain program's by a relative error of at most 0.022.
Values may be sent and summed in bfloat16 or wider, within the bound.
A program may use at most 128 MiB of HBM per device.

v0:
```python
import math
import jax
import jax.numpy as jnp
from jax import lax
from jax.sharding import PartitionSpec as P


def per_device(queries, keys, values, cum_gate, residual, w_out, gain, w_up, w_down):
    tok_rows, width = queries.shape
    heads_here = cum_gate.shape[1]
    head_size = width // heads_here
    score_scale = head_size ** (-0.5)
    row_offset = lax.axis_index("sp") * tok_rows
    query_heads = queries.reshape(tok_rows, heads_here, head_size)
    query_pos = row_offset + jnp.arange(tok_rows, dtype=jnp.int32)
    all_gates = lax.all_gather(cum_gate, "sp", axis=0, tiled=True)
    initial = (
        jnp.full((tok_rows, heads_here), -1e30, jnp.float32),
        jnp.zeros((tok_rows, heads_here), jnp.float32),
        jnp.zeros((tok_rows, heads_here, head_size), jnp.float32),
    )
    carried = initial
    key_rows = lax.all_gather(keys, "sp", axis=0, tiled=True)
    value_rows = lax.all_gather(values, "sp", axis=0, tiled=True)
    row_count = key_rows.shape[0]
    span_rows = math.gcd(row_count, 2048)
    block_count = row_count // span_rows
    key_blocks = key_rows.reshape(block_count, span_rows, heads_here, head_size)
    value_blocks = value_rows.reshape(block_count, span_rows, heads_here, head_size)
    first_pos = jnp.arange(block_count, dtype=jnp.int32) * span_rows

    def absorb_block(running, packed):
        running_max, running_sum, accumulated = running
        key_blk, value_blk, block_start = packed
        gate_blk = lax.dynamic_slice_in_dim(all_gates, block_start, span_rows, 0)
        scores = jnp.einsum(
            "qhd,khd->qhk", query_heads, key_blk, preferred_element_type=jnp.float32
        )
        scores = scores * score_scale + cum_gate[:, :, None] - gate_blk.T[None, :, :]
        key_pos = block_start + jnp.arange(span_rows, dtype=jnp.int32)
        scores = jnp.where(key_pos[None, None, :] <= query_pos[:, None, None], scores, -1e30)
        new_max = jnp.maximum(running_max, jnp.max(scores, axis=-1))
        rescale = jnp.exp(running_max - new_max)
        weights = jnp.exp(scores - new_max[:, :, None])
        running_sum = running_sum * rescale + jnp.sum(weights, axis=-1)
        product = jnp.einsum(
            "qhk,khd->qhd",
            weights.astype(jnp.bfloat16),
            value_blk,
            preferred_element_type=jnp.float32,
        )
        accumulated = accumulated * rescale[:, :, None] + product
        return ((new_max, running_sum, accumulated), None)

    carried, _ = lax.scan(absorb_block, carried, (key_blocks, value_blocks, first_pos))
    running_max, running_sum, accumulated = carried
    attended = (accumulated / running_sum[:, :, None]).reshape(tok_rows, width).astype(jnp.bfloat16)
    mine = lax.all_to_all(attended, "tp", split_axis=0, concat_axis=1, tiled=True)
    projected = jnp.dot(mine, w_out, preferred_element_type=jnp.float32)
    residual_sum = residual.astype(jnp.float32) + projected
    mean_square = jnp.mean(residual_sum * residual_sum, axis=-1, keepdims=True)
    normed = (residual_sum * lax.rsqrt(mean_square + 1e-06) * gain).astype(jnp.bfloat16)
    normed_all = lax.all_gather(normed, "tp", axis=0, tiled=True)
    up_proj = jnp.dot(
        normed_all,
        lax.all_gather(w_up, "sp", axis=0, tiled=True),
        preferred_element_type=jnp.float32,
    )
    hidden = jnp.square(jax.nn.relu(up_proj)).astype(jnp.bfloat16)
    down_whole = lax.all_gather(w_down, "sp", axis=1, tiled=True)
    rounded = jnp.dot(hidden, down_whole, preferred_element_type=jnp.float32).astype(jnp.bfloat16)
    branch_out = lax.psum_scatter(
        lax.optimization_barrier(rounded).astype(jnp.float32).astype(jnp.bfloat16),
        "tp",
        scatter_dimension=0,
        tiled=True,
    ).astype(jnp.float32)
    return (residual_sum + branch_out).astype(jnp.bfloat16)


def solution(mesh):
    return jax.shard_map(
        per_device,
        mesh=mesh,
        in_specs=(
            P("sp", "tp"),
            P("sp", "tp"),
            P("sp", "tp"),
            P("sp", "tp"),
            P(("sp", "tp"), None),
            P(),
            P(),
            P("sp", "tp"),
            P("tp", "sp"),
        ),
        out_specs=P(("sp", "tp"), None),
        check_vma=False,
    )
```

profile of v0, /device:TPU:0, one launch (start us, length us, event | category | flops | bytes accessed | tf_op | source)
XLA Modules:
  0.0 501.9 jit_solution(15590965651173478988)
XLA Ops:
  8.1 1.1 copy.17
  9.4 32.7 %all_gather.19 = f32[4096,2]{0,1:T(2,128)S(1)} all-gather(f32[512,2]{0,1:T(2,128)} %param.14), channel_id=1, replica_groups=mesh['sp'=8,'tp'=4] {'sp'}, dimensions={0}, use_global_device_ids=true | all-gather | bytes 36864 | tf_op jit(solution)/shard_map/all_gather | solution.py:16
  42.0 19.4 %all-gather.6.cloned.1.call-done = bf16[4096,256]{1,0:T(8,128)(2,1)} async-done(((bf16[512,256]{1,0:T(8,128)(2,1)}), bf16[4096,256]{1,0:T(8,128)(2,1)}) %all-gather.6.cloned.1.call-update) | async-done | bytes 2097168 | tf_op jit(solution)/shard_map/all_gather | solution.py:23
  61.4 4.0 reshape.62
  65.4 45.8 %all-gather.8.cloned.1.call-done = bf16[4096,256]{1,0:T(8,128)(2,1)} async-done(((bf16[512,256]{1,0:T(8,128)(2,1)}), bf16[4096,256]{1,0:T(8,128)(2,1)}) %all-gather.8.cloned.1.call-update) | async-done | bytes 2097168 | tf_op jit(solution)/shard_map/all_gather | solution.py:24
  111.2 4.0 reshape.64
  115.2 45.9 %while.15 = (s32[]{:T(128)}, f32[512,2]{0,1:T(2,128)S(1)}, f32[512,2]{0,1:T(2,128)S(1)}, f32[512,2,128]{0,2,1:T(8,128)}, s32[2]{0:T(128)S(1)}, /*index=5*/bf16[2...) while((s32[]{:T(128)}, f32[512,2]{0,1:T(2,128)S(1)}, ...), condition=%wide.region_3.4_spmd.clone, body=%wide.region_0.3_spmd.clone.sunk | while | flops 1110842880 | bytes 39239884 | solution.py:55
  118.9 2.7 constant_dynamic-slice_fusion.3
  121.6 4.6 fusion.40
  126.2 4.8 fusion.42
  131.8 6.2 %fusion.44 = f32[512,2,128]{0,2,1:T(8,128)} fusion(f32[2,2048,512]{2,1,0:T(8,128)} %get-tuple-element.231, f32[512,2]{0,1:T(2,128)S(1)} %fusion.41, f32[2,2048]{1,0:T(2,128)S(1)} %dynamic-slice_bitcast_fusion.2, f32[512,2]{0,1:T(2,128)S(1)} %get-tuple-element.270, pred[512,2048]{0,1:T(8,128)(4,1)S(1)} %broadcast_compare_fusion.2, ...), kind=kOutput, calls=%fused_computation.12.clone.1 | convolution fusion | flops 549847040 | bytes 11563009 | tf_op jit(solution)/shard_map/while/body/eval_jaxpr/qhk,khd->qhd/dot_general | solution.py:46
  141.8 2.7 constant_dynamic-slice_fusion.3
  144.5 4.6 fusion.40
  149.1 4.8 fusion.42
  154.7 6.4 %fusion.44 = f32[512,2,128]{0,2,1:T(8,128)} fusion(f32[2,2048,512]{2,1,0:T(8,128)} %get-tuple-element.231, f32[512,2]{0,1:T(2,128)S(1)} %fusion.41, f32[2,2048]{1,0:T(2,128)S(1)} %dynamic-slice_bitcast_fusion.2, f32[512,2]{0,1:T(2,128)S(1)} %get-tuple-element.270, pred[512,2048]{0,1:T(8,128)(4,1)S(1)} %broadcast_compare_fusion.2, ...), kind=kOutput, calls=%fused_computation.12.clone.1 | convolution fusion | flops 549847040 | bytes 11563009 | tf_op jit(solution)/shard_map/while/body/eval_jaxpr/qhk,khd->qhd/dot_general | solution.py:46
  161.1 1.1 divide_convert_fusion
  162.4 8.5 %all_to_all.16 = bf16[4,128,256]{2,1,0:T(8,128)(2,1)S(1)} all-to-all(bf16[4,128,256]{2,1,0:T(8,128)(2,1)S(1)} %copy.24), channel_id=1, replica_groups=mesh['sp'=8,'tp'=4] {'tp'}, dimensions={0} | all-to-all | bytes 524288 | tf_op jit(solution)/shard_map/all_to_all | solution.py:58
  171.1 3.1 multiply_reduce_fusion
  176.7 19.0 %all-gather.10.cloned.1.call-done = bf16[512,2048]{1,0:T(8,128)(2,1)} async-done(((bf16[128,2048]{1,0:T(8,128)(2,1)}), bf16[512,2048]{1,0:T(8,128)(2,1)}) %all-gather.10.cloned.1.call-update) | async-done | bytes 2097168 | tf_op jit(solution)/shard_map/all_gather | solution.py:63
  195.6 126.5 %all-gather.12.cloned.1.call-done = bf16[2048,2048]{1,0:T(8,128)(2,1)} async-done(((bf16[256,2048]{1,0:T(8,128)(2,1)}), bf16[2048,2048]{1,0:T(8,128)(2,1)}) %all-gather.12.cloned.1.call-update) | async-done | bytes 8388624 | tf_op jit(solution)/shard_map/all_gather | solution.py:66
  322.1 125.0 %all-gather.14.cloned.1.call-done = bf16[2048,2048]{1,0:T(8,128)(2,1)} async-done(((bf16[2048,256]{1,0:T(8,128)(2,1)}), bf16[2048,2048]{1,0:T(8,128)(2,1)}) %all-gather.14.cloned.1.call-update) | async-done | bytes 8388624 | tf_op jit(solution)/shard_map/all_gather | solution.py:70
  447.1 16.5 %convolution_convert_fusion = bf16[512,2048]{1,0:T(8,128)(2,1)} fusion(bf16[2048,2048]{1,0:T(8,128)(2,1)} %all-gather.14.cloned.1.call-done, bf16[512,2048]{1,0:T(8,128)(2,1)} %all-gather.10.cloned.1.call-done, bf16[2048,2048]{1,0:T(8,128)(2,1)} %all-gather.12.cloned.1.call-done), kind=kOutput, calls=%fused_computation.30 | convolution fusion | flops 8594128896 | bytes 20971520 | tf_op jit(solution)/shard_map/dot_general | solution.py:71
  463.7 29.5 %reduce-scatter.2.cloned.1.call-done = bf16[128,2048]{1,0:T(8,128)(2,1)} async-done(((bf16[512,2048]{1,0:T(8,128)(2,1)}), bf16[128,2048]{1,0:T(8,128)(2,1)}) %reduce-scatter.2.cloned.1.call-update) | async-done | bytes 524304 | tf_op jit(solution)/shard_map/reduce_scatter | solution.py:72
  493.2 1.9 add_convert_fusion
  (44 shorter events, 10.1 us)
Async XLA Ops:
  6.5 108.6 %copy-start = (f32[512,2]{0,1:T(2,128)S(1)}, f32[512,2]{0,1:T(2,128)}, u32[]{:S(2)}) copy-start(f32[512,2]{0,1:T(2,128)} %param.14) | copy-start | bytes 12292
  6.5 54.9 %all-gather.6.cloned.1.call-start = ((), (), s32[]{:S(2)}) async-start(), calls=%async_computation.2 | async-start | bytes 2359296 | tf_op jit(solution)/shard_map/all_gather | solution.py:23
  7.3 103.9 %all-gather.8.cloned.1.call-start = ((), (), s32[]{:S(2)}) async-start(), calls=%async_computation.3 | async-start | bytes 2359296 | tf_op jit(solution)/shard_map/all_gather | solution.py:24
  8.0 187.6 %all-gather.10.cloned.1.call-start = ((), (), s32[]{:S(2)}) async-start(), calls=%async_computation.4 | async-start | bytes 2621440 | tf_op jit(solution)/shard_map/all_gather | solution.py:63
  161.1 13.2 %copy-start.1 = (f32[2048]{0:T(1024)S(1)}, f32[2048]{0:T(1024)}, u32[]{:S(2)}) copy-start(f32[2048]{0:T(1024)} %param.17) | copy-start | bytes 24580
  175.3 146.8 %all-gather.12.cloned.1.call-start = ((), (), s32[]{:S(2)}) async-start(), calls=%async_computation.5 | async-start | bytes 9437184 | tf_op jit(solution)/shard_map/all_gather | solution.py:66
  175.8 271.3 %all-gather.14.cloned.1.call-start = ((), (), s32[]{:S(2)}) async-start(), calls=%async_computation.6 | async-start | bytes 9437184 | tf_op jit(solution)/shard_map/all_gather | solution.py:70
  176.4 316.7 %reduce-scatter.2.cloned.1.call-start = ((), (), s32[]{:S(2)}) async-start(), calls=%async_computation.7 | async-start | bytes 2621440 | tf_op jit(solution)/shard_map/reduce_scatter | solution.py:72
Sparse Core Ops, SparseCore 0:
  9.5 51.9 all-gather.5
  63.5 47.6 all-gather.7
  175.4 20.1 all-gather.9
  197.6 124.4 all-gather.11
  324.0 123.1 all-gather.13
  463.8 29.3 reduce-scatter.1
where the time goes:
time: 502 us
  waiting for transfers between devices  368 us (73%)
  matrix products  41.4 us (8%)
  blocking collectives  41.2 us (8%)
  local copies, waits for them, and re-layouts  18 us (4%)
  other arithmetic  16.3 us (3%)
  between operations  13.6 us (3%)
    all_gather x1, waiting for transfers between devices, per_device(): lax.all_gather(w_up, 'sp', axis=0, tiled=True)  126 us
    all_gather x1, waiting for transfers between devices, per_device(): down_whole = lax.all_gather(w_down, 'sp', axis=1, tiled=True)  125 us
    all_gather x1, waiting for transfers between devices, per_device(): value_rows = lax.all_gather(values, 'sp', axis=0, tiled=True)  45.8 us
    all_gather x1, blocking collectives, per_device(): all_gates = lax.all_gather(cum_gate, 'sp', axis=0, tiled=True)  32.7 us
    reduce_scatter x1, waiting for transfers between devices, per_device(): lax.psum_scatter(lax.optimization_barrier(rounded).astype(jnp.float32).as...  29.5 us
    all_gather x1, waiting for transfers between devices, per_device(): key_rows = lax.all_gather(keys, 'sp', axis=0, tiled=True)  19.4 us
    all_gather x1, waiting for transfers between devices, per_device(): normed_all = lax.all_gather(normed, 'tp', axis=0, tiled=True)  19 us
    dot_general x1, matrix products, per_device(): jnp.dot(hidden, down_whole, preferred_element_type=jnp.float32)  16.5 us
  transfers between devices with their start and end apart: 6, of which 6 were waited for; matrix products, arithmetic and copies ran while one was open for 1% of the time, Pallas kernels for 0%

commit v1 on v0

--- a/solution.py
+++ b/solution.py
@@ -20,8 +20,11 @@
         jnp.zeros((tok_rows, heads_here, head_size), jnp.float32),
     )
     carried = initial
-    key_rows = lax.all_gather(keys, "sp", axis=0, tiled=True)
-    value_rows = lax.all_gather(values, "sp", axis=0, tiled=True)
+    key_rows, value_rows = jnp.split(
+        lax.all_gather(jnp.concatenate([keys, values], axis=1), "sp", axis=0, tiled=True),
+        [keys.shape[1]],
+        axis=1,
+    )
     row_count = key_rows.shape[0]
     span_rows = math.gcd(row_count, 2048)
     block_count = row_count // span_rows

time: 502 us -> 483 us (0.962)
  waiting for transfers between devices: 368 us -> 343 us
    all_gather x2 -> x1, waiting for transfers between devices: 65.1 us -> 42.2 us  [per_device(): lax.all_gather(jnp.concatenate([keys, values], axis=1), 'sp', axis=0, til...]
  transfers between devices with their start and end apart: 6 -> 5, of which waited for: 6 -> 5; matrix products, arithmetic and copies ran while one was open for 1% -> 0% of each run, Pallas kernels for 0% -> 0%
where the time goes in v1:
time: 483 us; the launch traced here: 482 us
  waiting for transfers between devices  343 us (71%)
  blocking collectives  41.8 us (9%)
  matrix products  41.4 us (9%)
  local copies, waits for them, and re-layouts  20 us (4%)
  other arithmetic  18.3 us (4%)
  between operations  13.2 us (3%)
    all_gather x1, waiting for transfers between devices, per_device(): down_whole = lax.all_gather(w_down, 'sp', axis=1, tiled=True)  127 us
    all_gather x1, waiting for transfers between devices, per_device(): lax.all_gather(w_up, 'sp', axis=0, tiled=True)  125 us
    all_gather x1, waiting for transfers between devices, per_device(): lax.all_gather(jnp.concatenate([keys, values], axis=1), 'sp', axis=0, til...  42.2 us
    all_gather x1, blocking collectives, per_device(): all_gates = lax.all_gather(cum_gate, 'sp', axis=0, tiled=True)  33.2 us
    reduce_scatter x1, waiting for transfers between devices, per_device(): lax.psum_scatter(lax.optimization_barrier(rounded).astype(jnp.float32).as...  29.5 us
    all_gather x1, waiting for transfers between devices, per_device(): normed_all = lax.all_gather(normed, 'tp', axis=0, tiled=True)  18.8 us
    dot_general x1, matrix products, per_device(): jnp.dot(hidden, down_whole, preferred_element_type=jnp.float32)  16.5 us
    dot_general x2, matrix products, absorb_block(): jnp.einsum('qhk,khd->qhd', weights.astype(jnp.bfloat16), value_blk, prefe...  12.6 us
  transfers between devices with their start and end apart: 5, of which 5 were waited for; matrix products, arithmetic and copies ran while one was open for 0% of the time, Pallas kernels for 0%

profile of v1, /device:TPU:0, one launch (start us, length us, event | category | flops | bytes accessed | tf_op | source)
XLA Modules:
  0.0 482.3 jit_solution(15498138060287067180)
XLA Ops:
  6.5 1.9 pad_maximum_fusion
  9.8 33.2 %all_gather.16 = f32[4096,2]{0,1:T(2,128)S(1)} all-gather(f32[512,2]{0,1:T(2,128)} %param.14), channel_id=1, replica_groups=mesh['sp'=8,'tp'=4] {'sp'}, dimensions={0}, use_global_device_ids=true | all-gather | bytes 36864 | tf_op jit(solution)/shard_map/all_gather | solution.py:16
  43.0 42.2 %all-gather.5.cloned.1.call-done = bf16[4096,512]{1,0:T(8,128)(2,1)} async-done(((bf16[512,512]{1,0:T(8,128)(2,1)}), bf16[4096,512]{1,0:T(8,128)(2,1)}) %all-gather.5.cloned.1.call-update) | async-done | bytes 4194320 | tf_op jit(solution)/shard_map/all_gather | solution.py:24
  85.2 3.8 fusion.23
  89.0 4.0 reshape.62
  93.0 2.1 reshape.64
  95.1 46.5 %while.15 = (s32[]{:T(128)}, f32[512,2]{0,1:T(2,128)S(1)}, f32[512,2]{0,1:T(2,128)S(1)}, f32[512,2,128]{0,2,1:T(8,128)}, s32[2]{0:T(128)S(1)}, /*index=5*/bf16[2...) while((s32[]{:T(128)}, f32[512,2]{0,1:T(2,128)S(1)}, ...), condition=%wide.region_3.4_spmd.clone, body=%wide.region_0.3_spmd.clone.sunk | while | flops 1110842880 | bytes 39239884 | solution.py:58
  99.1 2.7 constant_dynamic-slice_fusion.3
  101.8 4.6 fusion.41
  106.4 4.8 fusion.43
  112.0 6.2 %fusion.45 = f32[512,2,128]{0,2,1:T(8,128)} fusion(f32[2,2048,512]{2,1,0:T(8,128)} %get-tuple-element.233, f32[512,2]{0,1:T(2,128)S(1)} %fusion.42, f32[2,2048]{1,0:T(2,128)S(1)} %dynamic-slice_bitcast_fusion.2, f32[512,2]{0,1:T(2,128)S(1)} %get-tuple-element.272, pred[512,2048]{0,1:T(8,128)(4,1)S(1)} %broadcast_compare_fusion.2, ...), kind=kOutput, calls=%fused_computation.12.clone.1 | convolution fusion | flops 549847040 | bytes 11563009 | tf_op jit(solution)/shard_map/while/body/eval_jaxpr/qhk,khd->qhd/dot_general | solution.py:49
  122.3 2.7 constant_dynamic-slice_fusion.3
  125.0 4.6 fusion.41
  129.6 4.8 fusion.43
  135.2 6.4 %fusion.45 = f32[512,2,128]{0,2,1:T(8,128)} fusion(f32[2,2048,512]{2,1,0:T(8,128)} %get-tuple-element.233, f32[512,2]{0,1:T(2,128)S(1)} %fusion.42, f32[2,2048]{1,0:T(2,128)S(1)} %dynamic-slice_bitcast_fusion.2, f32[512,2]{0,1:T(2,128)S(1)} %get-tuple-element.272, pred[512,2048]{0,1:T(8,128)(4,1)S(1)} %broadcast_compare_fusion.2, ...), kind=kOutput, calls=%fused_computation.12.clone.1 | convolution fusion | flops 549847040 | bytes 11563009 | tf_op jit(solution)/shard_map/while/body/eval_jaxpr/qhk,khd->qhd/dot_general | solution.py:49
  141.6 1.1 divide_convert_fusion
  142.9 8.5 %all_to_all.16 = bf16[4,128,256]{2,1,0:T(8,128)(2,1)S(1)} all-to-all(bf16[4,128,256]{2,1,0:T(8,128)(2,1)S(1)} %copy.24), channel_id=1, replica_groups=mesh['sp'=8,'tp'=4] {'tp'}, dimensions={0} | all-to-all | bytes 524288 | tf_op jit(solution)/shard_map/all_to_all | solution.py:61
  151.6 3.1 multiply_reduce_fusion
  157.3 18.8 %all-gather.7.cloned.1.call-done = bf16[512,2048]{1,0:T(8,128)(2,1)} async-done(((bf16[128,2048]{1,0:T(8,128)(2,1)}), bf16[512,2048]{1,0:T(8,128)(2,1)}) %all-gather.7.cloned.1.call-update) | async-done | bytes 2097168 | tf_op jit(solution)/shard_map/all_gather | solution.py:66
  176.1 127.0 %all-gather.11.cloned.1.call-done = bf16[2048,2048]{1,0:T(8,128)(2,1)} async-done(((bf16[2048,256]{1,0:T(8,128)(2,1)}), bf16[2048,2048]{1,0:T(8,128)(2,1)}) %all-gather.11.cloned.1.call-update) | async-done | bytes 8388624 | tf_op jit(solution)/shard_map/all_gather | solution.py:73
  303.1 124.7 %all-gather.9.cloned.1.call-done = bf16[2048,2048]{1,0:T(8,128)(2,1)} async-done(((bf16[256,2048]{1,0:T(8,128)(2,1)}), bf16[2048,2048]{1,0:T(8,128)(2,1)}) %all-gather.9.cloned.1.call-update) | async-done | bytes 8388624 | tf_op jit(solution)/shard_map/all_gather | solution.py:69
  427.8 16.5 %convolution_convert_fusion = bf16[512,2048]{1,0:T(8,128)(2,1)} fusion(bf16[2048,2048]{1,0:T(8,128)(2,1)} %all-gather.11.cloned.1.call-done, bf16[512,2048]{1,0:T(8,128)(2,1)} %all-gather.7.cloned.1.call-done, bf16[2048,2048]{1,0:T(8,128)(2,1)} %all-gather.9.cloned.1.call-done), kind=kOutput, calls=%fused_computation.30 | convolution fusion | flops 8594128896 | bytes 20971520 | tf_op jit(solution)/shard_map/dot_general | solution.py:74
  444.3 29.5 %reduce-scatter.2.cloned.1.call-done = bf16[128,2048]{1,0:T(8,128)(2,1)} async-done(((bf16[512,2048]{1,0:T(8,128)(2,1)}), bf16[128,2048]{1,0:T(8,128)(2,1)}) %reduce-scatter.2.cloned.1.call-update) | async-done | bytes 524304 | tf_op jit(solution)/shard_map/reduce_scatter | solution.py:75
  473.8 1.9 add_convert_fusion
  (43 shorter events, 10.2 us)
Async XLA Ops:
  6.5 78.7 %all-gather.5.cloned.1.call-start = ((), (), s32[]{:S(2)}) async-start(), calls=%async_computation.2 | async-start | bytes 4718592 | tf_op jit(solution)/shard_map/all_gather | solution.py:24
  8.4 167.7 %all-gather.7.cloned.1.call-start = ((), (), s32[]{:S(2)}) async-start(), calls=%async_computation.3 | async-start | bytes 2621440 | tf_op jit(solution)/shard_map/all_gather | solution.py:66
  43.0 52.0 %copy-start = (f32[512,2]{0,1:T(2,128)S(1)}, f32[512,2]{0,1:T(2,128)}, u32[]{:S(2)}) copy-start(f32[512,2]{0,1:T(2,128)} %param.14) | copy-start | bytes 12292
  141.6 13.2 %copy-start.1 = (f32[2048]{0:T(1024)S(1)}, f32[2048]{0:T(1024)}, u32[]{:S(2)}) copy-start(f32[2048]{0:T(1024)} %param.17) | copy-start | bytes 24580
  155.7 147.4 %all-gather.11.cloned.1.call-start = ((), (), s32[]{:S(2)}) async-start(), calls=%async_computation.5 | async-start | bytes 9437184 | tf_op jit(solution)/shard_map/all_gather | solution.py:73
  156.5 271.3 %all-gather.9.cloned.1.call-start = ((), (), s32[]{:S(2)}) async-start(), calls=%async_computation.4 | async-start | bytes 9437184 | tf_op jit(solution)/shard_map/all_gather | solution.py:69
  157.1 316.7 %reduce-scatter.2.cloned.1.call-start = ((), (), s32[]{:S(2)}) async-start(), calls=%async_computation.6 | async-start | bytes 2621440 | tf_op jit(solution)/shard_map/reduce_scatter | solution.py:75
Sparse Core Ops, SparseCore 0:
  9.5 75.7 all-gather.4
  155.9 20.1 all-gather.6
  178.1 124.9 all-gather.10
  305.1 122.6 all-gather.8
  444.4 29.3 reduce-scatter.1
